TPU v7x, 32 devices: a whole 2x2x4 slice. The times are simulated.
32 devices in a mesh: sp: 16 (over z, y, core), tp: 2 (over x).
Axes of the slice: x: 2, y: 2, z: 4, core: 2. Of those that a mesh axis runs over, the one named last changes fastest.
Arguments:
- tokens: bfloat16 [4096, 2048], P(('sp', 'tp')), may hold values from -6 to 6
- norm_gain: float32 [2048], replicated, may hold values from 0.1 to 1.9
- w_query: bfloat16 [2048, 1024], P('sp', 'tp'), may hold values from -0.125 to 0.125
- w_forget: bfloat16 [2048, 1024], P('sp', 'tp'), may hold values from -0.125 to 0.125
- w_input: bfloat16 [2048, 1024], P('sp', 'tp'), may hold values from -0.125 to 0.125
- w_outgate: bfloat16 [2048, 1024], P('sp', 'tp'), may hold values from -0.125 to 0.125
- w_bgate: bfloat16 [2048, 1024], P('sp', 'tp'), may hold values from -0.125 to 0.125
- w_cgate: bfloat16 [2048, 1024], P('sp', 'tp'), may hold values from -0.125 to 0.125
- w_value: bfloat16 [2048, 1024], P('sp', 'tp'), may hold values from -0.125 to 0.125
- floor_gap: float32 [8, 128], P('tp'), may hold values from 0 to 0.06
- extra_decay: float32 [4096, 8], P('sp', 'tp'), may hold values from -1 to 0
- start_state: float32 [8, 128, 128], P('tp'), may hold values from -0.109375 to 0.109375
- state_gain: float32 [128], replicated, may hold values from 0.1 to 1.9
- conv_taps: float32 [3, 1024], P(None, 'tp'), may hold values from -3 to 3
- out_rec: bfloat16 [1024, 2048], P('tp', 'sp'), may hold values from -0.125 to 0.125
- out_conv: bfloat16 [1024, 2048], P('tp', 'sp'), may hold values from -0.125 to 0.125
Outputs:
- mixed_sum: bfloat16 [4096, 2048], P(('sp', 'tp'))
All inputs are finite; a program needn't handle non-finite values.
Results may differ from a plain program's by a relative error of at most 0.018.
Values may be sent and summed in bfloat16 or wider, within the bound.
A program may use at most 64 MiB of HBM per device.

v0:
```python
import jax
import jax.numpy as jnp
from jax import lax
from jax.sharding import PartitionSpec as P

BLOCK = 64
eps = 1e-06
highest_precision = lax.Precision.HIGHEST


def prefix(value, axis, join, neutral):
    count, mine = (lax.axis_size(axis), lax.axis_index(axis))
    pieces = jax.tree.map(lambda part: lax.all_gather(part, axis), value)
    so_far = jax.tree.map(
        lambda part, zero: jnp.full_like(part, 0) + jnp.asarray(zero, part.dtype), value, neutral
    )

    def hop(position, so_far):
        longer = join(so_far, jax.tree.map(lambda part: part[position], pieces))
        return jax.tree.map(lambda new, old: jnp.where(position < mine, new, old), longer, so_far)

    return lax.fori_loop(0, count - 1, hop, so_far)


def shifted(block, axis, distance):
    devices = range(lax.axis_size(axis))
    route = [(i - distance, i) for i in devices if i - distance in devices]
    return lax.ppermute(block, axis, route)


def rms_scale(values):
    return lax.rsqrt(jnp.mean(values * values, axis=-1, keepdims=True) + eps)


def local_blocks(queries, write_in, inputs, log_keep, block_len):
    length, head_count, address_feature_count = queries.shape
    value_dim = inputs.shape[-1]
    blocks_count = length // block_len

    def blocked(tensor):
        return tensor.reshape(blocks_count, block_len, head_count, tensor.shape[-1]).transpose(
            0, 2, 1, 3
        )

    def unblock(tensor):
        return tensor.transpose(0, 2, 1, 3).reshape(length, head_count, tensor.shape[-1])

    causal = (jnp.arange(block_len)[:, None] >= jnp.arange(block_len)[None, :])[None, :, :, None]

    def advance(carried, pieces):
        memory_state, offset = carried
        query_block, write_blk, input_block, keep_blk = pieces
        running_state = jnp.cumsum(keep_blk, axis=1)
        spread = running_state[:, :, None, :] - running_state[:, None, :, :]
        decays = jnp.where(causal, jnp.exp(jnp.minimum(spread, 0.0)), 0.0)
        scores = jnp.sum(query_block[:, :, None, :] * write_blk[:, None, :, :] * decays, axis=-1)
        final_output = jnp.einsum(
            "qcp,qpi->qci",
            query_block * jnp.exp(running_state),
            memory_state,
            precision=highest_precision,
        )
        final_output = final_output + jnp.einsum(
            "hts,hsv->htv", scores, input_block, precision=highest_precision
        )
        lifted_state = query_block * jnp.exp(running_state + offset[:, None, :])
        final_state = running_state[:, -1, :]
        weighted_value = write_blk * jnp.exp(final_state[:, None, :] - running_state)
        memory_state = memory_state * jnp.exp(final_state)[:, :, None] + jnp.einsum(
            "euz,eul->ezl", weighted_value, input_block, precision=highest_precision
        )
        return ((memory_state, offset + final_state), (final_output, lifted_state))

    initial = (
        jnp.zeros((head_count, address_feature_count, value_dim), jnp.float32),
        jnp.zeros((head_count, address_feature_count), jnp.float32),
    )
    finals, outputs = lax.scan(
        advance, initial, (blocked(queries), blocked(write_in), blocked(inputs), blocked(log_keep))
    )
    return (unblock(outputs[0]), unblock(outputs[1]), finals[0], jnp.exp(finals[1]))


def chain(earlier, later):
    return (earlier[0] * later[0], earlier[1] * later[0][:, :, None] + later[1])


def on_device(
    tokens,
    norm_gain,
    w_query,
    w_forget,
    w_input,
    w_outgate,
    w_bgate,
    w_cgate,
    w_value,
    floor_gap,
    extra_decay,
    start_state,
    state_gain,
    conv_taps,
    out_rec,
    out_conv,
):
    tokens_f = tokens.astype(jnp.float32)
    normed = (tokens_f * rms_scale(tokens_f) * norm_gain).astype(jnp.bfloat16)
    weights = (w_query, w_forget, w_input, w_outgate, w_bgate, w_cgate, w_value)
    whole_weights = (
        lax.all_gather(w_query, "sp", axis=0, tiled=True),
        lax.all_gather(w_forget, "sp", axis=0, tiled=True),
        lax.all_gather(w_input, "sp", axis=0, tiled=True),
        lax.all_gather(w_outgate, "sp", axis=0, tiled=True),
        lax.all_gather(w_bgate, "sp", axis=0, tiled=True),
        lax.all_gather(w_cgate, "sp", axis=0, tiled=True),
        lax.all_gather(w_value, "sp", axis=0, tiled=True),
    )

    def project(shard_rows):
        return jnp.concatenate(
            [
                jnp.dot(shard_rows, matrix, preferred_element_type=jnp.float32).astype(jnp.bfloat16)
                for matrix in whole_weights
            ],
            axis=1,
        )

    joined = project(lax.all_gather(normed, "tp", axis=0, tiled=True))
    borders = [0]
    for matrix in weights:
        borders.append(borders[-1] + matrix.shape[1])
    projected = [joined[:, borders[number] : borders[number + 1]] for number in range(len(weights))]
    query_raw, forget_raw, input_raw, outgate_raw, bgate_raw, cgate_raw, value_raw = projected
    length = query_raw.shape[0]
    head_count, address_feature_count = floor_gap.shape
    value_dim = start_state.shape[2]
    queries = jax.nn.silu(query_raw.astype(jnp.float32)).reshape(
        length, head_count, address_feature_count
    )
    write_in = floor_gap[None] * jax.nn.sigmoid(-forget_raw.astype(jnp.float32)).reshape(
        length, head_count, address_feature_count
    )
    log_keep = jnp.log1p(-write_in) + extra_decay[:, :, None]
    inputs = input_raw.astype(jnp.float32).reshape(length, head_count, value_dim)
    output_list, lifted_state, memory_state, kept = local_blocks(
        queries, write_in, inputs, log_keep, BLOCK
    )
    before_keep, before_memory = prefix(
        (kept, memory_state), "sp", chain, (jnp.ones_like(kept), jnp.zeros_like(memory_state))
    )
    carried_hidden_prior = start_state * before_keep[:, :, None] + before_memory
    blended_state = output_list + jnp.einsum(
        "sqa,qar->sqr", lifted_state, carried_hidden_prior, precision=highest_precision
    )
    gate_out = jax.nn.silu(outgate_raw.astype(jnp.float32)).reshape(length, head_count, value_dim)
    rec_out = (
        (blended_state * rms_scale(blended_state) * state_gain * gate_out)
        .reshape(length, head_count * value_dim)
        .astype(jnp.bfloat16)
    )
    rim_rows = jnp.stack([cgate_raw[length - 2 :], value_raw[length - 2 :]])
    before_rim = shifted(rim_rows, "sp", 1)
    convolution_gate_widened = jnp.concatenate([before_rim[0], cgate_raw], axis=0).astype(
        jnp.float32
    )
    value_ext = jnp.concatenate([before_rim[1], value_raw], axis=0).astype(jnp.float32)
    gated = convolution_gate_widened * value_ext
    conv_out = (
        conv_taps[0] * gated[:length]
        + conv_taps[1] * gated[1 : length + 1]
        + conv_taps[2] * gated[2:]
    )
    short_out = (bgate_raw.astype(jnp.float32) * conv_out).astype(jnp.bfloat16)
    rec_weight, conv_weight = (
        lax.all_gather(out_rec, "sp", axis=1, tiled=True),
        lax.all_gather(out_conv, "sp", axis=1, tiled=True),
    )
    product = jnp.dot(rec_out, rec_weight, preferred_element_type=jnp.float32)
    return lax.psum_scatter(
        (product + jnp.dot(short_out, conv_weight, preferred_element_type=jnp.float32)).astype(
            jnp.bfloat16
        ),
        "tp",
        scatter_dimension=0,
        tiled=True,
    )


def solution(mesh):
    placed = (
        P(("sp", "tp"), None),
        P(),
        P("sp", "tp"),
        P("sp", "tp"),
        P("sp", "tp"),
        P("sp", "tp"),
        P("sp", "tp"),
        P("sp", "tp"),
        P("sp", "tp"),
        P("tp", None),
        P("sp", "tp"),
        P("tp", None, None),
        P(),
        P(None, "tp"),
        P("tp", "sp"),
        P("tp", "sp"),
    )
    return jax.shard_map(
        on_device, mesh=mesh, in_specs=placed, out_specs=P(("sp", "tp"), None), check_vma=False
    )
```

profile of v0, /device:TPU:0, one launch (start us, length us, event | category | flops | bytes accessed | tf_op | source)
XLA Modules:
  0.0 498.2 jit_solution(12257426766689084749)
XLA Ops:
  6.5 1.2 fusion.37
  7.8 2.0 fusion.39
  14.0 20.0 %all-gather.15.cloned.1.call-done = bf16[256,2048]{1,0:T(8,128)(2,1)} async-done(((bf16[128,2048]{1,0:T(8,128)(2,1)}), bf16[256,2048]{1,0:T(8,128)(2,1)}) %all-gather.15.cloned.1.call-update) | async-done | bytes 1048592 | tf_op jit(solution)/shard_map/all_gather | solution.py:128
  34.0 43.6 %all-gather.19.cloned.1.call-done = bf16[2048,512]{1,0:T(8,128)(2,1)} async-done(((bf16[128,512]{1,0:T(8,128)(2,1)}), bf16[2048,512]{1,0:T(8,128)(2,1)}) %all-gather.19.cloned.1.call-update) | async-done | bytes 2097168 | tf_op jit(solution)/shard_map/all_gather | solution.py:112
  77.7 2.6 fusion.31
  80.5 39.6 %all-gather.21.cloned.1.call-done = bf16[2048,512]{1,0:T(8,128)(2,1)} async-done(((bf16[128,512]{1,0:T(8,128)(2,1)}), bf16[2048,512]{1,0:T(8,128)(2,1)}) %all-gather.21.cloned.1.call-update) | async-done | bytes 2097168 | tf_op jit(solution)/shard_map/all_gather | solution.py:110
  120.0 2.4 divide_multiply_fusion.1
  122.6 39.7 %all-gather.17.cloned.1.call-done = bf16[2048,512]{1,0:T(8,128)(2,1)} async-done(((bf16[128,512]{1,0:T(8,128)(2,1)}), bf16[2048,512]{1,0:T(8,128)(2,1)}) %all-gather.17.cloned.1.call-update) | async-done | bytes 2097168 | tf_op jit(solution)/shard_map/all_gather | solution.py:111
  162.2 3.2 fusion.30
  165.4 1.2 reshape.81
  167.0 22.6 %while.33 = (s32[]{:T(128)}, f32[4,128,128]{2,1,0:T(8,128)S(1)}, f32[4,128]{1,0:T(4,128)S(1)}, f32[4,4,64,128]{3,2,0,1:T(8,128)}, f32[4,4,64,128]{3,2,0,1:T(8,12...) while((s32[]{:T(128)}, f32[4,128,128]{2,1,0:T(8,128)S(1)}, ...), condition=%wide.region_4.5_spmd.clone, body=%wide.region_1.4_spmd.clone.sunk | while | flops 140923904 | bytes 4028565 | solution.py:78
  167.3 3.4 multiply_reduce_fusion.3
  172.9 3.4 multiply_reduce_fusion.3
  178.6 3.4 multiply_reduce_fusion.3
  184.2 3.4 multiply_reduce_fusion.3
  192.6 11.9 %all-gather.31.cloned.1.call-done = bf16[2048,512]{1,0:T(8,128)(2,1)} async-done(((bf16[128,512]{1,0:T(8,128)(2,1)}), bf16[2048,512]{1,0:T(8,128)(2,1)}) %all-gather.31.cloned.1.call-update) | async-done | bytes 2097168 | tf_op jit(solution)/shard_map/all_gather | solution.py:116
  204.5 2.6 convolution_convert_fusion
  207.1 39.6 %all-gather.29.cloned.1.call-done = bf16[2048,512]{1,0:T(8,128)(2,1)} async-done(((bf16[128,512]{1,0:T(8,128)(2,1)}), bf16[2048,512]{1,0:T(8,128)(2,1)}) %all-gather.29.cloned.1.call-update) | async-done | bytes 2097168 | tf_op jit(solution)/shard_map/all_gather | solution.py:115
  246.7 2.3 convolution_convert_fusion.1
  249.1 2.3 collective-permute-start
  251.3 37.7 %all-gather.23.cloned.1.call-done = bf16[2048,512]{1,0:T(8,128)(2,1)} async-done(((bf16[128,512]{1,0:T(8,128)(2,1)}), bf16[2048,512]{1,0:T(8,128)(2,1)}) %all-gather.23.cloned.1.call-update) | async-done | bytes 2097168 | tf_op jit(solution)/shard_map/all_gather | solution.py:113
  289.1 3.2 divide_multiply_fusion
  292.2 19.4 %all-gather.2 = f32[16,4,128]{2,1,0:T(4,128)S(1)} all-gather(f32[1,4,128]{2,1,0:T(4,128)S(1)} %exponential_bitcast_fusion), channel_id=2, replica_groups=mesh['sp'=16,'tp'=2] {'sp'}, dimensions={0}, use_global_device_ids=true | all-gather | bytes 34816 | tf_op jit(solution)/shard_map/all_gather | solution.py:13
  311.8 1.2 copy.52
  313.1 1.1 convert_multiply_fusion.2
  314.2 26.2 %all-gather.35.cloned.1.call-done = f32[64,128,128]{2,1,0:T(8,128)} async-done(((f32[4,128,128]{2,1,0:T(8,128)}), f32[64,128,128]{2,1,0:T(8,128)}) %all-gather.35.cloned.1.call-update) | async-done | bytes 4194320 | tf_op jit(solution)/shard_map/all_gather | solution.py:13
  340.4 18.0 %while.34 = (s32[]{:T(128)}, f32[4,128]{1,0:T(4,128)S(1)}, f32[4,128,128]{2,1,0:T(8,128)S(1)}, s32[]{:T(128)}, f32[16,4,128]{2,1,0:T(4,128)S(1)}, /*index=5*/f32[16,4,128,128]{3,2,1,0:T(8,128)}, s32[]{:T(128)}, s32[]{:T(128)}) while((s32[]{:T(128)}, f32[4,128]{1,0:T(4,128)S(1)}, f32[4,128,128]{2,1,0:T(8,128)S(1)}, s32[]{:T(128)}, ...), condition=%wide.region_6.7_spmd.clone, body=%wide.region_5.6_spmd.clone.sunk | while | flops 263684 | bytes 796787 | solution.py:22
  340.5 1.1 fusion.94
  341.7 1.2 fusion.94
  342.9 1.2 fusion.94
  344.1 1.2 fusion.94
  345.3 1.2 fusion.94
  346.5 1.2 fusion.94
  347.7 1.2 fusion.94
  348.9 1.2 fusion.94
  350.1 1.2 fusion.94
  351.3 1.2 fusion.94
  352.5 1.2 fusion.94
  353.7 1.2 fusion.94
  354.9 1.2 fusion.94
  356.1 1.2 fusion.94
  357.3 1.2 fusion.94
  359.4 22.9 %all-gather.25.cloned.1.call-done = bf16[512,2048]{1,0:T(8,128)(2,1)} async-done(((bf16[512,128]{1,0:T(8,128)(2,1)}), bf16[512,2048]{1,0:T(8,128)(2,1)}) %all-gather.25.cloned.1.call-update) | async-done | bytes 2097168 | tf_op jit(solution)/shard_map/all_gather | solution.py:175
  382.2 2.3 fusion.53
  384.5 40.3 %all-gather.27.cloned.1.call-done = bf16[2048,512]{1,0:T(8,128)(2,1)} async-done(((bf16[128,512]{1,0:T(8,128)(2,1)}), bf16[2048,512]{1,0:T(8,128)(2,1)}) %all-gather.27.cloned.1.call-update) | async-done | bytes 2097168 | tf_op jit(solution)/shard_map/all_gather | solution.py:114
  424.8 42.0 %all-gather.33.cloned.1.call-done = bf16[512,2048]{1,0:T(8,128)(2,1)} async-done(((bf16[512,128]{1,0:T(8,128)(2,1)}), bf16[512,2048]{1,0:T(8,128)(2,1)}) %all-gather.33.cloned.1.call-update) | async-done | bytes 2097168 | tf_op jit(solution)/shard_map/all_gather | solution.py:176
  466.7 4.9 fusion.25
  471.7 19.6 %reduce-scatter.2.cloned.1.call-done = bf16[128,2048]{1,0:T(8,128)(2,1)} async-done(((bf16[256,2048]{1,0:T(8,128)(2,1)}), bf16[128,2048]{1,0:T(8,128)(2,1)}) %reduce-scatter.2.cloned.1.call-update) | async-done | bytes 524304 | tf_op jit(solution)/shard_map/reduce_scatter | solution.py:179
  (123 shorter events, 17.7 us)
Async XLA Ops:
  6.5 7.4 %copy-start.7 = (f32[256,4]{0,1:T(4,128)S(1)}, f32[256,4]{0,1:T(4,128)}, u32[]{:S(2)}) copy-start(f32[256,4]{0,1:T(4,128)} %param.30) | copy-start | bytes 12292
  6.5 27.5 %all-gather.15.cloned.1.call-start = ((), (), s32[]{:S(2)}) async-start(), calls=%async_computation.1 | async-start | bytes 1572864 | tf_op jit(solution)/shard_map/all_gather | solution.py:128
  9.8 67.8 %all-gather.19.cloned.1.call-start = ((), (), s32[]{:S(2)}) async-start(), calls=%async_computation.3 | async-start | bytes 2228224 | tf_op jit(solution)/shard_map/all_gather | solution.py:112
  10.6 109.4 %all-gather.21.cloned.1.call-start = ((), (), s32[]{:S(2)}) async-start(), calls=%async_computation.4 | async-start | bytes 2228224 | tf_op jit(solution)/shard_map/all_gather | solution.py:110
  11.3 150.9 %all-gather.17.cloned.1.call-start = ((), (), s32[]{:S(2)}) async-start(), calls=%async_computation.2 | async-start | bytes 2228224 | tf_op jit(solution)/shard_map/all_gather | solution.py:111
  11.9 192.6 %all-gather.31.cloned.1.call-start = ((), (), s32[]{:S(2)}) async-start(), calls=%async_computation.9 | async-start | bytes 2228224 | tf_op jit(solution)/shard_map/all_gather | solution.py:116
  12.5 234.2 %all-gather.29.cloned.1.call-start = ((), (), s32[]{:S(2)}) async-start(), calls=%async_computation.8 | async-start | bytes 2228224 | tf_op jit(solution)/shard_map/all_gather | solution.py:115
  13.1 276.0 %all-gather.23.cloned.1.call-start = ((), (), s32[]{:S(2)}) async-start(), calls=%async_computation.5 | async-start | bytes 2228224 | tf_op jit(solution)/shard_map/all_gather | solution.py:113
  13.8 326.6 %all-gather.35.cloned.1.call-start = ((), (), s32[]{:S(2)}) async-start(), calls=%async_computation.12 | async-start | bytes 4456448 | tf_op jit(solution)/shard_map/all_gather | solution.py:13
  34.0 86.0 %copy-start.1 = (bf16[256,2048]{1,0:T(8,128)(2,1)S(1)}, bf16[256,2048]{1,0:T(8,128)(2,1)}, u32[]{:S(2)}) copy-start(bf16[256,2048]{1,0:T(8,128)(2,1)} %all-gather.15.cloned.1.call-done) | copy-start | bytes 3145732
  165.4 1.4 copy-start.8
  167.0 25.5 %copy-start.6 = (f32[3,512]{1,0:T(4,128)S(1)}, f32[3,512]{1,0:T(4,128)}, u32[]{:S(2)}) copy-start(f32[3,512]{1,0:T(4,128)} %param.33) | copy-start | bytes 18436
  189.7 0.7 copy-start
  190.4 56.3 %copy-start.2 = (bf16[256,2048]{1,0:T(8,128)(2,1)S(1)}, bf16[256,2048]{1,0:T(8,128)(2,1)}, u32[]{:S(2)}) copy-start(bf16[256,2048]{1,0:T(8,128)(2,1)} %all-gather.15.cloned.1.call-done) | copy-start | bytes 3145732
  190.4 191.8 %all-gather.25.cloned.1.call-start = ((), (), s32[]{:S(2)}) async-start(), calls=%async_computation.6 | async-start | bytes 2228224 | tf_op jit(solution)/shard_map/all_gather | solution.py:175
  191.1 233.7 %all-gather.27.cloned.1.call-start = ((), (), s32[]{:S(2)}) async-start(), calls=%async_computation.7 | async-start | bytes 2228224 | tf_op jit(solution)/shard_map/all_gather | solution.py:114
  191.7 275.0 %all-gather.33.cloned.1.call-start = ((), (), s32[]{:S(2)}) async-start(), calls=%async_computation.10 | async-start | bytes 2228224 | tf_op jit(solution)/shard_map/all_gather | solution.py:176
  192.5 298.9 %reduce-scatter.2.cloned.1.call-start = ((), (), s32[]{:S(2)}) async-start(), calls=%async_computation.11 | async-start | bytes 1572864 | tf_op jit(solution)/shard_map/reduce_scatter | solution.py:179
  249.0 43.2 %copy-start.4 = (bf16[256,512]{1,0:T(8,128)(2,1)}, bf16[256,512]{1,0:T(8,128)(2,1)S(1)}, u32[]{:S(2)}) copy-start(bf16[256,512]{1,0:T(8,128)(2,1)S(1)} %convolution_convert_fusion.1) | copy-start | bytes 786436
  249.0 62.6 %copy-start.3 = (f32[4,4,64,128]{3,2,0,1:T(8,128)S(1)}, f32[4,4,64,128]{3,2,0,1:T(8,128)}, u32[]{:S(2)}) copy-start(f32[4,4,64,128]{3,2,0,1:T(8,128)} %get-tuple-element.170) | copy-start | bytes 1572868
  249.1 64.0 %collective-permute-start = (bf16[2,2,512]{2,1,0:T(2,128)(2,1)S(1)}, bf16[2,2,512]{2,1,0:T(2,128)(2,1)S(1)}, u32[]{:S(2)}, u32[]{:S(2)}) collective-permute-start(bf16[2,2,512]{2,1,0:T(2,128)(2,1)S(1)} %pad_maximum_fusion), channel_id=1, source_target_pairs={{0,2},{2,4},{4,6},{6,8},{8,10},{10,12},{12,14},{14,16},{16,18},{18... | collective-permute-start | bytes 12296 | tf_op jit(solution)/shard_map/ppermute | solution.py:28
  314.2 44.2 %copy-start.5 = (f32[4,128,128]{2,1,0:T(8,128)S(1)}, f32[4,128,128]{2,1,0:T(8,128)}, u32[]{:S(2)}) copy-start(f32[4,128,128]{2,1,0:T(8,128)} %param.31) | copy-start | bytes 786436
  358.4 0.8 copy-start.9
Sparse Core Ops, SparseCore 0:
  10.0 23.9 all-gather.14
  36.2 41.4 all-gather.18
  79.8 40.1 all-gather.20
  122.0 40.1 all-gather.16
  164.3 40.1 all-gather.30
  206.5 40.1 all-gather.28
  248.9 40.1 all-gather.22
  291.2 49.1 all-gather.34
  342.6 39.5 all-gather.24
  384.2 40.5 all-gather.26
  427.0 39.7 all-gather.32
  471.8 19.4 reduce-scatter.1
where the time goes:
time: 499 us; the launch traced here: 498 us
  waiting for transfers between devices  389 us (78%)
  other arithmetic  36.6 us (7%)
  matrix products  32 us (6%)
  blocking collectives  19.4 us (4%)
  between operations  13.9 us (3%)
    all_gather x1, waiting for transfers between devices, on_device(): lax.all_gather(w_input, 'sp', axis=0, tiled=True)  43.6 us
    all_gather x1, waiting for transfers between devices, on_device(): lax.all_gather(out_conv, 'sp', axis=1, tiled=True)  42 us
    all_gather x1, waiting for transfers between devices, on_device(): lax.all_gather(w_bgate, 'sp', axis=0, tiled=True)  40.3 us
    all_gather x1, waiting for transfers between devices, on_device(): lax.all_gather(w_forget, 'sp', axis=0, tiled=True)  39.7 us
    all_gather x1, waiting for transfers between devices, on_device(): lax.all_gather(w_cgate, 'sp', axis=0, tiled=True)  39.6 us
    all_gather x1, waiting for transfers between devices, on_device(): lax.all_gather(w_query, 'sp', axis=0, tiled=True)  39.6 us
    all_gather x1, waiting for transfers between devices, on_device(): lax.all_gather(w_outgate, 'sp', axis=0, tiled=True)  37.7 us
    all_gather x1, waiting for transfers between devices, prefix(): pieces = jax.tree.map(lambda part: lax.all_gather(part, axis), value)  26.2 us
  transfers between devices with their start and end apart: 13, of which 12 were waited for; matrix products, arithmetic and copies ran while one was open for 13% of the time, Pallas kernels for 0%

commit v1 on v0

--- a/solution.py
+++ b/solution.py
@@ -6,6 +6,13 @@
 BLOCK = 64
 eps = 1e-06
 highest_precision = lax.Precision.HIGHEST
+
+
+def sectors_remake(raw, a_name, on_dim):
+    return jnp.concatenate(
+        jax.lax.all_to_all(jnp.stack(jax.lax.axis_size(a_name) * [raw], axis=0), a_name, 0, 0),
+        axis=on_dim,
+    )
 
 
 def prefix(value, axis, join, neutral):
@@ -109,7 +116,7 @@
     whole_weights = (
         lax.all_gather(w_query, "sp", axis=0, tiled=True),
         lax.all_gather(w_forget, "sp", axis=0, tiled=True),
-        lax.all_gather(w_input, "sp", axis=0, tiled=True),
+        sectors_remake(w_input, "sp", 0),
         lax.all_gather(w_outgate, "sp", axis=0, tiled=True),
         lax.all_gather(w_bgate, "sp", axis=0, tiled=True),
         lax.all_gather(w_cgate, "sp", axis=0, tiled=True),

time: 499 us -> 467 us (0.936)
  waiting for transfers between devices: 389 us -> 348 us
  starting transfers between devices: 2.69 us -> 10.2 us
    all_gather x1 -> x0, waiting for transfers between devices: 43.6 us -> none  [on_device(): lax.all_gather(w_input, 'sp', axis=0, tiled=True)]
    all_to_all x0 -> x1, waiting for transfers between devices: none -> 32.9 us  [sectors_remake(): jax.lax.all_to_all(jnp.stack(jax.lax.axis_size(a_name) * [raw], axis=0),...]
    all_gather x1, waiting for transfers between devices: 39.6 us -> 16.2 us  [on_device(): lax.all_gather(w_query, 'sp', axis=0, tiled=True)]
    all_gather x1, waiting for transfers between devices: 20 us -> 11.6 us  [on_device(): joined = project(lax.all_gather(normed, 'tp', axis=0, tiled=True))]
    all_to_all x0 -> x1, starting transfers between devices: none -> 7.55 us  [sectors_remake(): jax.lax.all_to_all(jnp.stack(jax.lax.axis_size(a_name) * [raw], axis=0),...]
  transfers between devices with their start and end apart: 13 -> 13, of which waited for: 12 -> 12; matrix products, arithmetic and copies ran while one was open for 13% -> 14% of each run, Pallas kernels for 0% -> 0%
where the time goes in v1:
time: 467 us; the launch traced here: 466 us
  waiting for transfers between devices  348 us (75%)
  other arithmetic  36.6 us (8%)
  matrix products  31.4 us (7%)
  blocking collectives  19.4 us (4%)
  between operations  13.6 us (3%)
  starting transfers between devices  10.2 us (2%)
  local copies, waits for them, and re-layouts  6.48 us (1%)
    all_gather x1, waiting for transfers between devices, on_device(): lax.all_gather(out_conv, 'sp', axis=1, tiled=True)  41.8 us
    all_gather x1, waiting for transfers between devices, on_device(): lax.all_gather(w_forget, 'sp', axis=0, tiled=True)  41 us
    all_gather x1, waiting for transfers between devices, on_device(): lax.all_gather(w_bgate, 'sp', axis=0, tiled=True)  40.4 us
    all_gather x1, waiting for transfers between devices, on_device(): lax.all_gather(w_cgate, 'sp', axis=0, tiled=True)  39.6 us
    all_gather x1, waiting for transfers between devices, on_device(): lax.all_gather(w_outgate, 'sp', axis=0, tiled=True)  37.6 us
    all_to_all x1, waiting for transfers between devices, sectors_remake(): jax.lax.all_to_all(jnp.stack(jax.lax.axis_size(a_name) * [raw], axis=0),...  32.9 us
    all_gather x1, waiting for transfers between devices, prefix(): pieces = jax.tree.map(lambda part: lax.all_gather(part, axis), value)  26.2 us
    all_gather x1, waiting for transfers between devices, on_device(): lax.all_gather(out_rec, 'sp', axis=1, tiled=True)  22.9 us
  transfers between devices with their start and end apart: 13, of which 12 were waited for; matrix products, arithmetic and copies ran while one was open for 14% of the time, Pallas kernels for 0%

profile of v1, /device:TPU:0, one launch (start us, length us, event | category | flops | bytes accessed | tf_op | source)
XLA Modules:
  0.0 466.3 jit_solution(9486304590346292088)
XLA Ops:
  6.5 1.3 fusion.37
  7.8 2.0 fusion.39
  12.5 1.6 stack.8
  14.1 7.5 %all-to-all-start = ((bf16[16,128,512]{2,1,0:T(8,128)(2,1)}), bf16[16,128,512]{2,1,0:T(8,128)(2,1)S(1)}, u32[]{:S(2)}, u32[]{:S(2)}) async-start(bf16[16,128,512]{2,1,0:T(8,128)(2,1)} %stack.8), calls=%async_computation | async-start | bytes 4194304 | tf_op jit(solution)/shard_map/all_to_all | solution.py:13
  22.4 11.6 %all-gather.14.cloned.1.call-done = bf16[256,2048]{1,0:T(8,128)(2,1)} async-done(((bf16[128,2048]{1,0:T(8,128)(2,1)}), bf16[256,2048]{1,0:T(8,128)(2,1)}) %all-gather.14.cloned.1.call-update) | async-done | bytes 1048592 | tf_op jit(solution)/shard_map/all_gather | solution.py:135
  34.0 32.9 %all-to-all-done = bf16[16,128,512]{2,1,0:T(8,128)(2,1)S(1)} async-done(((bf16[16,128,512]{2,1,0:T(8,128)(2,1)}), bf16[16,128,512]{2,1,0:T(8,128)(2,1)S(1)}, u32[]{:S(2)}, u32[]{:S(2)}) %all-to-all-start) | async-done | bytes 2097184 | tf_op jit(solution)/shard_map/all_to_all | solution.py:13
  66.9 2.8 fusion.31
  69.7 1.3 reshape.91
  71.0 16.2 %all-gather.18.cloned.1.call-done = bf16[2048,512]{1,0:T(8,128)(2,1)} async-done(((bf16[128,512]{1,0:T(8,128)(2,1)}), bf16[2048,512]{1,0:T(8,128)(2,1)}) %all-gather.18.cloned.1.call-update) | async-done | bytes 2097168 | tf_op jit(solution)/shard_map/all_gather | solution.py:117
  87.2 2.4 divide_multiply_fusion.1
  89.7 41.0 %all-gather.16.cloned.1.call-done = bf16[2048,512]{1,0:T(8,128)(2,1)} async-done(((bf16[128,512]{1,0:T(8,128)(2,1)}), bf16[2048,512]{1,0:T(8,128)(2,1)}) %all-gather.16.cloned.1.call-update) | async-done | bytes 2097168 | tf_op jit(solution)/shard_map/all_gather | solution.py:118
  130.8 2.4 fusion.30
  134.4 22.6 %while.33 = (s32[]{:T(128)}, f32[4,128,128]{2,1,0:T(8,128)S(1)}, f32[4,128]{1,0:T(4,128)S(1)}, f32[4,4,64,128]{3,2,0,1:T(8,128)}, f32[4,4,64,128]{3,2,0,1:T(8,12...) while((s32[]{:T(128)}, f32[4,128,128]{2,1,0:T(8,128)S(1)}, ...), condition=%wide.region_4.5_spmd.clone, body=%wide.region_1.4_spmd.clone.sunk | while | flops 140923904 | bytes 4028565 | solution.py:85
  134.6 3.4 multiply_reduce_fusion.3
  140.2 3.4 multiply_reduce_fusion.3
  145.9 3.4 multiply_reduce_fusion.3
  151.5 3.4 multiply_reduce_fusion.3
  159.9 13.2 %all-gather.28.cloned.1.call-done = bf16[2048,512]{1,0:T(8,128)(2,1)} async-done(((bf16[128,512]{1,0:T(8,128)(2,1)}), bf16[2048,512]{1,0:T(8,128)(2,1)}) %all-gather.28.cloned.1.call-update) | async-done | bytes 2097168 | tf_op jit(solution)/shard_map/all_gather | solution.py:123
  173.0 2.6 convolution_convert_fusion
  175.7 39.6 %all-gather.26.cloned.1.call-done = bf16[2048,512]{1,0:T(8,128)(2,1)} async-done(((bf16[128,512]{1,0:T(8,128)(2,1)}), bf16[2048,512]{1,0:T(8,128)(2,1)}) %all-gather.26.cloned.1.call-update) | async-done | bytes 2097168 | tf_op jit(solution)/shard_map/all_gather | solution.py:122
  215.3 2.3 convolution_convert_fusion.1
  217.6 2.3 collective-permute-start
  219.9 37.6 %all-gather.20.cloned.1.call-done = bf16[2048,512]{1,0:T(8,128)(2,1)} async-done(((bf16[128,512]{1,0:T(8,128)(2,1)}), bf16[2048,512]{1,0:T(8,128)(2,1)}) %all-gather.20.cloned.1.call-update) | async-done | bytes 2097168 | tf_op jit(solution)/shard_map/all_gather | solution.py:120
  257.5 3.2 divide_multiply_fusion
  260.6 19.4 %all-gather.2 = f32[16,4,128]{2,1,0:T(4,128)S(1)} all-gather(f32[1,4,128]{2,1,0:T(4,128)S(1)} %exponential_bitcast_fusion), channel_id=2, replica_groups=mesh['sp'=16,'tp'=2] {'sp'}, dimensions={0}, use_global_device_ids=true | all-gather | bytes 34816 | tf_op jit(solution)/shard_map/all_gather | solution.py:20
  280.2 1.2 copy.52
  282.6 26.2 %all-gather.32.cloned.1.call-done = f32[64,128,128]{2,1,0:T(8,128)} async-done(((f32[4,128,128]{2,1,0:T(8,128)}), f32[64,128,128]{2,1,0:T(8,128)}) %all-gather.32.cloned.1.call-update) | async-done | bytes 4194320 | tf_op jit(solution)/shard_map/all_gather | solution.py:20
  308.9 18.0 %while.34 = (s32[]{:T(128)}, f32[4,128]{1,0:T(4,128)S(1)}, f32[4,128,128]{2,1,0:T(8,128)S(1)}, s32[]{:T(128)}, f32[16,4,128]{2,1,0:T(4,128)S(1)}, /*index=5*/f32[16,4,128,128]{3,2,1,0:T(8,128)}, s32[]{:T(128)}, s32[]{:T(128)}) while((s32[]{:T(128)}, f32[4,128]{1,0:T(4,128)S(1)}, f32[4,128,128]{2,1,0:T(8,128)S(1)}, s32[]{:T(128)}, ...), condition=%wide.region_6.7_spmd.clone, body=%wide.region_5.6_spmd.clone.sunk | while | flops 263684 | bytes 796787 | solution.py:29
  310.1 1.2 fusion.94
  311.3 1.2 fusion.94
  312.5 1.2 fusion.94
  313.7 1.2 fusion.94
  314.9 1.2 fusion.94
  316.1 1.2 fusion.94
  317.3 1.2 fusion.94
  318.5 1.2 fusion.94
  319.7 1.2 fusion.94
  320.9 1.2 fusion.94
  322.1 1.2 fusion.94
  323.3 1.2 fusion.94
  324.5 1.2 fusion.94
  325.7 1.2 fusion.94
  327.8 22.9 %all-gather.22.cloned.1.call-done = bf16[512,2048]{1,0:T(8,128)(2,1)} async-done(((bf16[512,128]{1,0:T(8,128)(2,1)}), bf16[512,2048]{1,0:T(8,128)(2,1)}) %all-gather.22.cloned.1.call-update) | async-done | bytes 2097168 | tf_op jit(solution)/shard_map/all_gather | solution.py:182
  350.6 2.3 fusion.53
  352.9 40.4 %all-gather.24.cloned.1.call-done = bf16[2048,512]{1,0:T(8,128)(2,1)} async-done(((bf16[128,512]{1,0:T(8,128)(2,1)}), bf16[2048,512]{1,0:T(8,128)(2,1)}) %all-gather.24.cloned.1.call-update) | async-done | bytes 2097168 | tf_op jit(solution)/shard_map/all_gather | solution.py:121
  393.3 41.8 %all-gather.30.cloned.1.call-done = bf16[512,2048]{1,0:T(8,128)(2,1)} async-done(((bf16[512,128]{1,0:T(8,128)(2,1)}), bf16[512,2048]{1,0:T(8,128)(2,1)}) %all-gather.30.cloned.1.call-update) | async-done | bytes 2097168 | tf_op jit(solution)/shard_map/all_gather | solution.py:183
  435.1 4.9 %fusion.25 = bf16[256,2048]{1,0:T(8,128)(2,1)} fusion(f32[256,2048]{1,0:T(8,128)S(1)} %fusion.53, bf16[512,2048]{1,0:T(8,128)(2,1)} %all-gather.30.cloned.1.call-done, bf16[256,2048]{1,0:T(8,128)(2,1)} %all-gather.14.cloned.1.call-done, bf16[2048,512]{1,0:T(8,128)(2,1)} %all-gather.24.cloned.1.call-done, f32[258,512]{1,0:T(8,128)S(1)} %convert_multiply_fusion.2, ...), kind=kOutput, calls=%fused_computation.38 | convolution fusion | flops 1075970048 | bytes 9967616 | tf_op jit(solution)/shard_map/dot_general | solution.py:187
  440.1 19.6 %reduce-scatter.2.cloned.1.call-done = bf16[128,2048]{1,0:T(8,128)(2,1)} async-done(((bf16[256,2048]{1,0:T(8,128)(2,1)}), bf16[128,2048]{1,0:T(8,128)(2,1)}) %reduce-scatter.2.cloned.1.call-update) | async-done | bytes 524304 | tf_op jit(solution)/shard_map/reduce_scatter | solution.py:186
  (127 shorter events, 19.8 us)
Async XLA Ops:
  6.5 6.0 %copy-start.7 = (bf16[128,512]{1,0:T(8,128)(2,1)S(1)}, bf16[128,512]{1,0:T(8,128)(2,1)}, u32[]{:S(2)}) copy-start(bf16[128,512]{1,0:T(8,128)(2,1)} %param.24) | copy-start | bytes 393220
  6.5 27.5 %all-gather.14.cloned.1.call-start = ((), (), s32[]{:S(2)}) async-start(), calls=%async_computation.2 | async-start | bytes 1572864 | tf_op jit(solution)/shard_map/all_gather | solution.py:135
  9.9 77.3 %all-gather.18.cloned.1.call-start = ((), (), s32[]{:S(2)}) async-start(), calls=%async_computation.4 | async-start | bytes 2228224 | tf_op jit(solution)/shard_map/all_gather | solution.py:117
  10.6 120.1 %all-gather.16.cloned.1.call-start = ((), (), s32[]{:S(2)}) async-start(), calls=%async_computation.3 | async-start | bytes 2228224 | tf_op jit(solution)/shard_map/all_gather | solution.py:118
  11.4 161.7 %all-gather.28.cloned.1.call-start = ((), (), s32[]{:S(2)}) async-start(), calls=%async_computation.9 | async-start | bytes 2228224 | tf_op jit(solution)/shard_map/all_gather | solution.py:123
  11.9 203.3 %all-gather.26.cloned.1.call-start = ((), (), s32[]{:S(2)}) async-start(), calls=%async_computation.8 | async-start | bytes 2228224 | tf_op jit(solution)/shard_map/all_gather | solution.py:122
  14.1 8.2 %copy-start.9 = (f32[256,4]{0,1:T(4,128)S(1)}, f32[256,4]{0,1:T(4,128)}, u32[]{:S(2)}) copy-start(f32[256,4]{0,1:T(4,128)} %param.30) | copy-start | bytes 12292
  14.1 52.8 %all-to-all-start = ((bf16[16,128,512]{2,1,0:T(8,128)(2,1)}), bf16[16,128,512]{2,1,0:T(8,128)(2,1)S(1)}, u32[]{:S(2)}, u32[]{:S(2)}) async-start(bf16[16,128,512]{2,1,0:T(8,128)(2,1)} %stack.8), calls=%async_computation | async-start | bytes 4194304 | tf_op jit(solution)/shard_map/all_to_all | solution.py:13
  21.7 235.8 %all-gather.20.cloned.1.call-start = ((), (), s32[]{:S(2)}) async-start(), calls=%async_computation.5 | async-start | bytes 2228224 | tf_op jit(solution)/shard_map/all_gather | solution.py:120
  22.3 286.6 %all-gather.32.cloned.1.call-start = ((), (), s32[]{:S(2)}) async-start(), calls=%async_computation.12 | async-start | bytes 4456448 | tf_op jit(solution)/shard_map/all_gather | solution.py:20
  66.9 20.3 %copy-start.1 = (bf16[256,2048]{1,0:T(8,128)(2,1)S(1)}, bf16[256,2048]{1,0:T(8,128)(2,1)}, u32[]{:S(2)}) copy-start(bf16[256,2048]{1,0:T(8,128)(2,1)} %all-gather.14.cloned.1.call-done) | copy-start | bytes 3145732
  133.1 0.7 copy-start.10
  133.3 1.0 copy-start.3
  134.4 25.4 %copy-start.8 = (f32[3,512]{1,0:T(4,128)S(1)}, f32[3,512]{1,0:T(4,128)}, u32[]{:S(2)}) copy-start(f32[3,512]{1,0:T(4,128)} %param.33) | copy-start | bytes 18436
  156.9 0.7 copy-start
  157.7 57.6 %copy-start.2 = (bf16[256,2048]{1,0:T(8,128)(2,1)S(1)}, bf16[256,2048]{1,0:T(8,128)(2,1)}, u32[]{:S(2)}) copy-start(bf16[256,2048]{1,0:T(8,128)(2,1)} %all-gather.14.cloned.1.call-done) | copy-start | bytes 3145732
  157.7 192.9 %all-gather.22.cloned.1.call-start = ((), (), s32[]{:S(2)}) async-start(), calls=%async_computation.6 | async-start | bytes 2228224 | tf_op jit(solution)/shard_map/all_gather | solution.py:182
  158.4 234.9 %all-gather.24.cloned.1.call-start = ((), (), s32[]{:S(2)}) async-start(), calls=%async_computation.7 | async-start | bytes 2228224 | tf_op jit(solution)/shard_map/all_gather | solution.py:121
  159.2 276.0 %all-gather.30.cloned.1.call-start = ((), (), s32[]{:S(2)}) async-start(), calls=%async_computation.10 | async-start | bytes 2228224 | tf_op jit(solution)/shard_map/all_gather | solution.py:183
  159.7 300.0 %reduce-scatter.2.cloned.1.call-start = ((), (), s32[]{:S(2)}) async-start(), calls=%async_computation.11 | async-start | bytes 1572864 | tf_op jit(solution)/shard_map/reduce_scatter | solution.py:186
  217.5 43.1 %copy-start.5 = (bf16[256,512]{1,0:T(8,128)(2,1)}, bf16[256,512]{1,0:T(8,128)(2,1)S(1)}, u32[]{:S(2)}) copy-start(bf16[256,512]{1,0:T(8,128)(2,1)S(1)} %convolution_convert_fusion.1) | copy-start | bytes 786436
  217.6 62.5 %copy-start.4 = (f32[4,4,64,128]{3,2,0,1:T(8,128)S(1)}, f32[4,4,64,128]{3,2,0,1:T(8,128)}, u32[]{:S(2)}) copy-start(f32[4,4,64,128]{3,2,0,1:T(8,128)} %get-tuple-element.170) | copy-start | bytes 1572868
  217.6 63.9 %collective-permute-start = (bf16[2,2,512]{2,1,0:T(2,128)(2,1)S(1)}, bf16[2,2,512]{2,1,0:T(2,128)(2,1)S(1)}, u32[]{:S(2)}, u32[]{:S(2)}) collective-permute-start(bf16[2,2,512]{2,1,0:T(2,128)(2,1)S(1)} %pad_maximum_fusion), channel_id=1, source_target_pairs={{0,2},{2,4},{4,6},{6,8},{8,10},{10,12},{12,14},{14,16},{16,18},{18... | collective-permute-start | bytes 12296 | tf_op jit(solution)/shard_map/ppermute | solution.py:35
  282.6 44.2 %copy-start.6 = (f32[4,128,128]{2,1,0:T(8,128)S(1)}, f32[4,128,128]{2,1,0:T(8,128)}, u32[]{:S(2)}) copy-start(f32[4,128,128]{2,1,0:T(8,128)} %param.31) | copy-start | bytes 786436
  326.8 0.8 copy-start.11
Sparse Core Ops, SparseCore 0:
  10.0 23.9 all-gather.13
  36.2 50.9 all-gather.17
  89.3 41.3 all-gather.15
  132.8 40.2 all-gather.27
  175.0 40.1 all-gather.25
  217.3 40.1 all-gather.19
  259.6 49.1 all-gather.31
  311.0 39.5 all-gather.21
  352.8 40.5 all-gather.23
  395.4 39.7 all-gather.29
  440.2 19.4 reduce-scatter.1
